TPU v7x, 128 devices: a whole 4x4x4 slice. The times are simulated.
128 devices in a mesh: rep: 2 (over z_hi), fs: 32 (over z_lo, y, x), tp: 2 (over core).
Axes of the slice: x: 4, y: 4, z: 4 (z_hi: 2, z_lo: 2; z = z_hi * 2 + z_lo), core: 2. Of those that a mesh axis runs over, the one named last changes fastest.
Arguments:
- tokens: bfloat16 [256, 64, 2048], P('tp', ('rep', 'fs')), may hold values from -6 to 6
- mix_gain: float32 [2048], replicated, may hold values from 0.1 to 1.9
- value_weight: bfloat16 [2048, 1024], P('fs', 'tp'), may hold values from -0.125 to 0.125
- gate_weight: bfloat16 [2048, 1024], P('fs', 'tp'), may hold values from -0.125 to 0.125
- conv_taps: float32 [31, 1024], P(None, 'tp'), may hold values from -1 to 1
- head_gain: float32 [1024], P('tp'), may hold values from 0.1 to 1.9
- out_weight: bfloat16 [1024, 2048], P('tp', 'fs'), may hold values from -0.1875 to 0.1875
- ffn_gain: float32 [2048], replicated, may hold values from 0.1 to 1.9
- ffn_gate_weight: bfloat16 [2048, 3072], P('fs', 'tp'), may hold values from -0.125 to 0.125
- ffn_up_weight: bfloat16 [2048, 3072], P('fs', 'tp'), may hold values from -0.125 to 0.125
- down_weight: bfloat16 [3072, 2048], P('tp', 'fs'), may hold values from -0.109375 to 0.109375
Outputs:
- layer_out: bfloat16 [256, 64, 2048], P('tp', ('rep', 'fs'))
All inputs are finite; a program needn't handle non-finite values.
Results may differ from a plain program's by a relative error of at most 0.012.
Values may be sent and summed in bfloat16 or wider, within the bound.
No kernel may reach another device: no remote copies, remote signals or barrier semaphores. Data moves between devices by JAX's collectives and lax.ppermute only.
A program may use at most 128 MiB of HBM per device.

v0:
```python
import jax
import jax.numpy as jnp
from jax import lax
from jax.sharding import PartitionSpec as P

HEAD_DIM = 128
norm_eps = 1e-06
group_eps = 1e-05


def from_everyone(value, axis):
    count = lax.axis_size(axis)
    return lax.all_to_all(
        jnp.broadcast_to(value[None], (count, *value.shape)), axis, 0, 0, tiled=True
    )


def laid_out(parts, dim):
    lengths = list(parts.shape[1:])
    lengths[dim] *= parts.shape[0]
    return jnp.moveaxis(parts, 0, dim).reshape(lengths)


def gather_directly(value, axis, dim):
    parts = from_everyone(value, axis)
    return laid_out(parts, dim)


def sent_together(arrays, axis, dim, along):
    both = jnp.concatenate(arrays, axis=along)
    out, at, finished = (lax.all_gather(both, axis, axis=dim, tiled=True), 0, [])
    for a in arrays:
        finished.append(lax.slice_in_dim(out, at, at + a.shape[along], axis=along))
        at += a.shape[along]
    return tuple(finished)


def cut_along(value, dim, count):
    before, after = (value.shape[:dim], value.shape[dim + 1 :])
    return jnp.moveaxis(value.reshape(*before, count, -1, *after), dim, 0)


def sent_and_summed(value, axis, dim):
    parts = cut_along(value, dim, lax.axis_size(axis))
    arrived = lax.all_to_all(parts, axis, split_axis=0, concat_axis=0, tiled=True)
    return arrived.astype(jnp.float32).sum(axis=0)


def rms_scale(matrix, scales):
    return matrix * lax.rsqrt(jnp.mean(matrix * matrix, axis=-1, keepdims=True) + norm_eps) * scales


def body(
    tokens,
    mix_gain,
    value_weight,
    gate_weight,
    conv_taps,
    head_gain,
    out_weight,
    ffn_gain,
    ffn_gate_weight,
    ffn_up_weight,
    down_weight,
):
    local_len, seq_count, model_width = tokens.shape
    own_rows = local_len * seq_count
    whole_rows = gather_directly(tokens, "tp", 0)
    full_len = whole_rows.shape[0]
    normed = rms_scale(whole_rows.reshape(-1, model_width).astype(jnp.float32), mix_gain).astype(
        jnp.bfloat16
    )
    channels = value_weight.shape[1]
    pieces = sent_together((value_weight, gate_weight), "fs", 0, 1)
    sliced = normed
    value_rows = jnp.dot(sliced, pieces[0], preferred_element_type=jnp.float32)
    gate_rows = jnp.dot(sliced, pieces[1], preferred_element_type=jnp.float32)
    glu_rows = (
        (value_rows * jax.nn.sigmoid(gate_rows))
        .astype(jnp.bfloat16)
        .reshape(full_len, seq_count, channels)
    )
    kernel = conv_taps.shape[0]
    conved = lax.conv_general_dilated(
        glu_rows.astype(jnp.float32),
        conv_taps[:, None, :],
        (1,),
        [(kernel // 2, kernel // 2)],
        dimension_numbers=("WNC", "WIO", "WNC"),
        feature_group_count=channels,
        precision=lax.Precision.HIGHEST,
    )
    grouped = conved.reshape(full_len, seq_count, channels // HEAD_DIM, HEAD_DIM)
    head_mean = jnp.mean(grouped, axis=-1, keepdims=True)
    head_var = jnp.mean(jnp.square(grouped - head_mean), axis=-1, keepdims=True)
    scaled = (
        (grouped - head_mean) * lax.rsqrt(head_var + group_eps) * head_gain.reshape(-1, HEAD_DIM)
    )
    activated = jax.nn.silu(scaled).astype(jnp.bfloat16).reshape(-1, channels)
    out_columns = gather_directly(out_weight, "fs", 1)
    sliced = lax.slice_in_dim(activated, 0, own_rows * lax.axis_size("tp"), axis=0)
    mixed_rows = sent_and_summed(
        jnp.dot(sliced, out_columns, preferred_element_type=jnp.float32).astype(jnp.bfloat16),
        "tp",
        0,
    )
    residual = tokens.reshape(own_rows, model_width).astype(jnp.float32)
    middle = (residual + mixed_rows).astype(jnp.bfloat16)
    middle_whole = gather_directly(middle.reshape(local_len, seq_count, model_width), "tp", 0)
    normed_ffn = rms_scale(
        middle_whole.reshape(-1, model_width).astype(jnp.float32), ffn_gain
    ).astype(jnp.bfloat16)
    pieces = sent_together((ffn_gate_weight, ffn_up_weight), "fs", 0, 1)
    sliced = normed_ffn
    gate_part = jnp.dot(sliced, pieces[0], preferred_element_type=jnp.float32)
    up_part = jnp.dot(sliced, pieces[1], preferred_element_type=jnp.float32)
    hidden = (jax.nn.silu(gate_part) * up_part).astype(jnp.bfloat16)
    down_columns = lax.all_gather(down_weight, "fs", axis=1, tiled=True)
    sliced = hidden
    fed_rows = sent_and_summed(
        jnp.dot(sliced, down_columns, preferred_element_type=jnp.float32).astype(jnp.bfloat16),
        "tp",
        0,
    )
    layer_rows = (middle.astype(jnp.float32) + fed_rows).astype(jnp.bfloat16)
    return layer_rows.reshape(local_len, seq_count, model_width)


def solution(mesh):
    placed = (
        P("tp", ("rep", "fs"), None),
        P(),
        P("fs", "tp"),
        P("fs", "tp"),
        P(None, "tp"),
        P("tp"),
        P("tp", "fs"),
        P(),
        P("fs", "tp"),
        P("fs", "tp"),
        P("tp", "fs"),
    )
    return jax.shard_map(
        body, mesh=mesh, in_specs=placed, out_specs=P("tp", ("rep", "fs"), None), check_vma=False
    )
```

profile of v0, /device:TPU:1, one launch (start us, length us, event | category | flops | bytes accessed | tf_op | source)
XLA Modules:
  0.0 537.6 jit_solution(16612511845772567293)
XLA Ops:
  6.5 1.6 pad_maximum_fusion.1
  8.2 1.8 pad_maximum_fusion
  10.9 5.6 %all_to_all.25 = bf16[2,128,1,2048]{3,1,2,0:T(8,128)(2,1)S(1)} all-to-all(bf16[2,128,1,2048]{3,1,2,0:T(8,128)(2,1)S(1)} %broadcast_in_dim.11), channel_id=1, replica_groups=mesh['rep'=2,'fs'=32,'tp'=2] {'tp'}, dimensions={0} | all-to-all | bytes 2097152 | tf_op jit(solution)/shard_map/all_to_all | solution.py:13
  16.5 1.6 broadcast_in_dim.13
  18.1 8.6 %all-to-all-start.1 = ((bf16[32,512,64]{1,2,0:T(8,128)(2,1)}), bf16[32,512,64]{1,2,0:T(8,128)(2,1)S(1)}, u32[]{:S(2)}, u32[]{:S(2)}) async-start(bf16[32,512,64]{1,2,0:T(8,128)(2,1)} %broadcast_in_dim.13), calls=%async_computation.1 | async-start | bytes 4194304 | tf_op jit(solution)/shard_map/all_to_all | solution.py:13
  27.0 1.3 fusion.17
  28.4 130.0 %all-gather.4.cloned.1.call-done = bf16[2048,1024]{1,0:T(8,128)(2,1)} async-done(((bf16[64,1024]{1,0:T(8,128)(2,1)}), bf16[2048,1024]{1,0:T(8,128)(2,1)}) %all-gather.4.cloned.1.call-update) | async-done | bytes 4194320 | tf_op jit(solution)/shard_map/all_gather | solution.py:31
  158.3 2.8 fusion.35
  161.5 0.7 fusion.38
  162.9 1.3 convolution_select_fusion
  164.6 0.9 reshape.190
  165.5 1.1 slice.21
  166.7 1.0 reshape.180
  168.1 1.7 multiply_reduce_fusion.2
  169.8 0.8 fusion.51
  170.6 0.7 convolution_convert_fusion
  171.3 23.2 %all_to_all.26 = bf16[2,128,2048]{2,1,0:T(8,128)(2,1)S(1)} all-to-all(bf16[2,128,2048]{2,1,0:T(8,128)(2,1)S(1)} %bitcast.53), channel_id=1, replica_groups=mesh['rep'=2,'fs'=32,'tp'=2] {'tp'}, dimensions={0} | all-to-all | bytes 2097152 | tf_op jit(solution)/shard_map/all_to_all | solution.py:45
  195.0 4.6 all_to_all.27
  200.2 134.7 %all-gather.6.cloned.1.call-done = bf16[2048,3072]{1,0:T(8,128)(2,1)} async-done(((bf16[64,3072]{1,0:T(8,128)(2,1)}), bf16[2048,3072]{1,0:T(8,128)(2,1)}) %all-gather.6.cloned.1.call-update) | async-done | bytes 12582928 | tf_op jit(solution)/shard_map/all_gather | solution.py:31
  334.9 5.7 %fusion.2 = f32[256,1536]{1,0:T(8,128)} fusion(bf16[256,2048]{1,0:T(8,128)(2,1)S(1)} %fusion.15, bf16[2048,3072]{1,0:T(8,128)(2,1)} %all-gather.6.cloned.1.call-done), kind=kOutput, calls=%fused_computation.2 | convolution fusion | flops 1610612736 | bytes 8912896 | tf_op jit(solution)/shard_map/dot_general | solution.py:115
  340.7 155.1 %all-gather.8.cloned.1.call-done = bf16[1536,2048]{0,1:T(8,128)(2,1)} async-done(((bf16[1536,64]{0,1:T(8,128)(2,1)}), bf16[1536,2048]{0,1:T(8,128)(2,1)}) %all-gather.8.cloned.1.call-update) | async-done | bytes 6291472 | tf_op jit(solution)/shard_map/all_gather | solution.py:118
  495.7 8.8 %convolution_convert_fusion.1 = bf16[256,2048]{1,0:T(8,128)(2,1)S(1)} fusion(bf16[1536,2048]{0,1:T(8,128)(2,1)} %all-gather.8.cloned.1.call-done, bf16[256,2048]{1,0:T(8,128)(2,1)} %copy-done.3, bf16[2048,3072]{1,0:T(8,128)(2,1)} %all-gather.6.cloned.1.call-done, f32[256,1536]{1,0:T(8,128)} %fusion.2), kind=kOutput, calls=%fused_computation.7 | convolution fusion | flops 3224109056 | bytes 16252928 | tf_op jit(solution)/shard_map/dot_general | solution.py:121
  504.5 25.3 %all_to_all.28 = bf16[2,128,2048]{2,1,0:T(8,128)(2,1)S(1)} all-to-all(bf16[2,128,2048]{2,1,0:T(8,128)(2,1)S(1)} %bitcast.54), channel_id=1, replica_groups=mesh['rep'=2,'fs'=32,'tp'=2] {'tp'}, dimensions={0} | all-to-all | bytes 2097152 | tf_op jit(solution)/shard_map/all_to_all | solution.py:45
  530.1 1.0 fusion.42
  (48 shorter events, 4.3 us)
Async XLA Ops:
  6.5 156.0 %copy-start = (f32[31,512]{1,0:T(8,128)S(1)}, f32[31,512]{1,0:T(8,128)}, u32[]{:S(2)}) copy-start(f32[31,512]{1,0:T(8,128)} %param.15) | copy-start | bytes 190468
  6.5 4.2 copy-start.1
  6.5 151.8 %all-gather.4.cloned.1.call-start = ((), (), s32[]{:S(2)}) async-start(), calls=%async_computation.5 | async-start | bytes 4325376 | tf_op jit(solution)/shard_map/all_gather | solution.py:31
  8.2 326.8 %all-gather.6.cloned.1.call-start = ((), (), s32[]{:S(2)}) async-start(), calls=%async_computation.6 | async-start | bytes 12976128 | tf_op jit(solution)/shard_map/all_gather | solution.py:31
  10.0 6.5 %copy-start.5 = (bf16[512,64]{0,1:T(8,128)(2,1)S(1)}, bf16[512,64]{0,1:T(8,128)(2,1)}, u32[]{:S(2)}) copy-start(bf16[512,64]{0,1:T(8,128)(2,1)} %param.17) | copy-start | bytes 196612
  10.0 485.7 %all-gather.8.cloned.1.call-start = ((), (), s32[]{:S(2)}) async-start(), calls=%async_computation.7 | async-start | bytes 6488064 | tf_op jit(solution)/shard_map/all_gather | solution.py:118
  18.1 8.9 %copy-start.6 = (f32[2048]{0:T(1024)S(1)}, f32[2048]{0:T(1024)}, u32[]{:S(2)}) copy-start(f32[2048]{0:T(1024)} %param.12) | copy-start | bytes 24580
  18.1 152.5 %all-to-all-start.1 = ((bf16[32,512,64]{1,2,0:T(8,128)(2,1)}), bf16[32,512,64]{1,2,0:T(8,128)(2,1)S(1)}, u32[]{:S(2)}, u32[]{:S(2)}) async-start(bf16[32,512,64]{1,2,0:T(8,128)(2,1)} %broadcast_in_dim.13), calls=%async_computation.1 | async-start | bytes 4194304 | tf_op jit(solution)/shard_map/all_to_all | solution.py:13
  28.4 132.8 %copy-start.4 = (bf16[256,2048]{1,0:T(8,128)(2,1)S(1)}, bf16[256,2048]{1,0:T(8,128)(2,1)}, u32[]{:S(2)}) copy-start(bf16[256,2048]{1,0:T(8,128)(2,1)} %fusion.17) | copy-start | bytes 3145732
  158.3 3.1 copy-start.9
  162.2 0.7 copy-start.10
  166.5 3.3 copy-start.8
  171.3 23.4 %copy-start.2 = (bf16[128,1,2048]{2,0,1:T(8,128)(2,1)S(1)}, bf16[128,1,2048]{2,0,1:T(8,128)(2,1)}, u32[]{:S(2)}) copy-start(bf16[128,1,2048]{2,0,1:T(8,128)(2,1)} %param.11) | copy-start | bytes 1572868
  194.8 5.1 copy-start.7
  200.2 140.4 %copy-start.3 = (bf16[256,2048]{1,0:T(8,128)(2,1)}, bf16[256,2048]{1,0:T(8,128)(2,1)S(1)}, u32[]{:S(2)}) copy-start(bf16[256,2048]{1,0:T(8,128)(2,1)S(1)} %fusion.15) | copy-start | bytes 3145732
Sparse Core Ops, SparseCore 0:
  9.0 149.3 all-gather.3
  160.0 174.9 all-gather.5
  336.6 159.1 all-gather.7
where the time goes:
time: 538 us
  waiting for transfers between devices  420 us (78%)
  blocking collectives  58.7 us (11%)
  matrix products  20.1 us (4%)
  between operations  13.4 us (2%)
  other arithmetic  9.93 us (2%)
  starting transfers between devices  8.72 us (2%)
  local copies, waits for them, and re-layouts  6.23 us (1%)
    all_gather x2, waiting for transfers between devices, sent_together(): lax.all_gather(both, axis, axis=dim, tiled=True)  265 us
    all_gather x1, waiting for transfers between devices, body(): down_columns = lax.all_gather(down_weight, 'fs', axis=1, tiled=True)  155 us
    all_to_all x2, blocking collectives, sent_and_summed(): lax.all_to_all(parts, axis, split_axis=0, concat_axis=0, tiled=True)  48.5 us
  transfers between devices with their start and end apart: 4, of which 3 were waited for; matrix products, arithmetic and copies ran while one was open for 4% of the time, Pallas kernels for 0%

commit v1 on v0

--- a/solution.py
+++ b/solution.py
@@ -6,6 +6,13 @@
 HEAD_DIM = 128
 norm_eps = 1e-06
 group_eps = 1e-05
+
+
+def search_heads(base_x, across):
+    mid_arr = lax.axis_size(across)
+    formed = jnp.stack([base_x] * mid_arr)
+    state_next = lax.all_to_all(formed, across, 0, 0)
+    return jnp.concatenate(state_next, 1)
 
 
 def from_everyone(value, axis):
@@ -115,7 +122,7 @@
     gate_part = jnp.dot(sliced, pieces[0], preferred_element_type=jnp.float32)
     up_part = jnp.dot(sliced, pieces[1], preferred_element_type=jnp.float32)
     hidden = (jax.nn.silu(gate_part) * up_part).astype(jnp.bfloat16)
-    down_columns = lax.all_gather(down_weight, "fs", axis=1, tiled=True)
+    down_columns = search_heads(down_weight, "fs")
     sliced = hidden
     fed_rows = sent_and_summed(
         jnp.dot(sliced, down_columns, preferred_element_type=jnp.float32).astype(jnp.bfloat16),

time: 538 us -> 457 us (0.85)
  waiting for transfers between devices: 420 us -> 333 us
  blocking collectives: 58.7 us -> 50.9 us
  starting transfers between devices: 8.72 us -> 16.1 us
    all_gather x1 -> x0, waiting for transfers between devices: 155 us -> none  [body(): down_columns = lax.all_gather(down_weight, 'fs', axis=1, tiled=True)]
    all_gather x2, waiting for transfers between devices: 265 us -> 333 us  [sent_together(): lax.all_gather(both, axis, axis=dim, tiled=True)]
    all_to_all x2, blocking collectives: 48.5 us -> 40.8 us  [sent_and_summed(): lax.all_to_all(parts, axis, split_axis=0, concat_axis=0, tiled=True)]
    all_to_all x0 -> x1, starting transfers between devices: none -> 7.41 us  [search_heads(): state_next = lax.all_to_all(formed, across, 0, 0)]
  transfers between devices with their start and end apart: 4 -> 4, of which waited for: 3 -> 2; matrix products, arithmetic and copies ran while one was open for 4% -> 7% of each run, Pallas kernels for 0% -> 0%
where the time goes in v1:
time: 457 us; the launch traced here: 456 us
  waiting for transfers between devices  333 us (73%)
  blocking collectives  50.9 us (11%)
  matrix products  20.6 us (5%)
  starting transfers between devices  16.1 us (4%)
  between operations  13.7 us (3%)
  other arithmetic  10.9 us (2%)
  local copies, waits for them, and re-layouts  10.6 us (2%)
    all_gather x2, waiting for transfers between devices, sent_together(): lax.all_gather(both, axis, axis=dim, tiled=True)  333 us
    all_to_all x2, blocking collectives, sent_and_summed(): lax.all_to_all(parts, axis, split_axis=0, concat_axis=0, tiled=True)  40.8 us
    all_to_all x2, blocking collectives, from_everyone(): lax.all_to_all(jnp.broadcast_to(value[None], (count, *value.shape)), axis...  10.2 us
  transfers between devices with their start and end apart: 4, of which 2 were waited for; matrix products, arithmetic and copies ran while one was open for 7% of the time, Pallas kernels for 0%

profile of v1, /device:TPU:1, one launch (start us, length us, event | category | flops | bytes accessed | tf_op | source)
XLA Modules:
  0.0 456.1 jit_solution(1332634045347429729)
XLA Ops:
  6.5 1.6 pad_maximum_fusion.1
  8.2 1.9 pad_maximum_fusion
  10.1 1.2 broadcast_in_dim.11
  11.3 5.6 %all_to_all.30 = bf16[2,128,1,2048]{3,1,2,0:T(8,128)(2,1)S(1)} all-to-all(bf16[2,128,1,2048]{3,1,2,0:T(8,128)(2,1)S(1)} %broadcast_in_dim.11), channel_id=1, replica_groups=mesh['rep'=2,'fs'=32,'tp'=2] {'tp'}, dimensions={0} | all-to-all | bytes 2097152 | tf_op jit(solution)/shard_map/all_to_all | solution.py:20
  16.9 1.6 broadcast_in_dim.13
  18.4 8.6 %all-to-all-start.1 = ((bf16[32,512,64]{1,2,0:T(8,128)(2,1)}), bf16[32,512,64]{1,2,0:T(8,128)(2,1)S(1)}, u32[]{:S(2)}, u32[]{:S(2)}) async-start(bf16[32,512,64]{1,2,0:T(8,128)(2,1)} %broadcast_in_dim.13), calls=%async_computation.1 | async-start | bytes 4194304 | tf_op jit(solution)/shard_map/all_to_all | solution.py:20
  27.4 1.3 fusion.17
  28.7 130.0 %all-gather.3.cloned.1.call-done = bf16[2048,1024]{1,0:T(8,128)(2,1)} async-done(((bf16[64,1024]{1,0:T(8,128)(2,1)}), bf16[2048,1024]{1,0:T(8,128)(2,1)}) %all-gather.3.cloned.1.call-update) | async-done | bytes 4194320 | tf_op jit(solution)/shard_map/all_gather | solution.py:38
  158.7 2.8 fusion.35
  163.3 1.3 convolution_select_fusion
  164.9 0.9 reshape.200
  165.8 1.1 slice.21
  167.1 1.0 reshape.188
  168.5 1.7 multiply_reduce_fusion.2
  171.7 23.4 %all_to_all.31 = bf16[2,128,2048]{2,1,0:T(8,128)(2,1)S(1)} all-to-all(bf16[2,128,2048]{2,1,0:T(8,128)(2,1)S(1)} %bitcast.56), channel_id=1, replica_groups=mesh['rep'=2,'fs'=32,'tp'=2] {'tp'}, dimensions={0} | all-to-all | bytes 2097152 | tf_op jit(solution)/shard_map/all_to_all | solution.py:52
  195.6 4.6 %all_to_all.32 = bf16[2,128,1,2048]{3,1,2,0:T(8,128)(2,1)S(1)} all-to-all(bf16[2,128,1,2048]{3,1,2,0:T(8,128)(2,1)S(1)} %broadcast_in_dim.14), channel_id=1, replica_groups=mesh['rep'=2,'fs'=32,'tp'=2] {'tp'}, dimensions={0} | all-to-all | bytes 2097152 | tf_op jit(solution)/shard_map/all_to_all | solution.py:20
  200.1 3.3 stack.2
  203.5 7.4 %all-to-all-start.4 = ((bf16[32,1536,64]{1,2,0:T(8,128)(2,1)}), bf16[32,1536,64]{1,2,0:T(8,128)(2,1)}, u32[]{:S(2)}, u32[]{:S(2)}) async-start(bf16[32,1536,64]{1,2,0:T(8,128)(2,1)} %stack.2), calls=%async_computation.4 | async-start | bytes 12582912 | tf_op jit(solution)/shard_map/all_to_all | solution.py:14
  211.2 1.3 fusion.15
  212.5 203.3 %all-gather.5.cloned.1.call-done = bf16[2048,3072]{1,0:T(8,128)(2,1)} async-done(((bf16[64,3072]{1,0:T(8,128)(2,1)}), bf16[2048,3072]{1,0:T(8,128)(2,1)}) %all-gather.5.cloned.1.call-update) | async-done | bytes 12582928 | tf_op jit(solution)/shard_map/all_gather | solution.py:38
  415.7 6.1 %fusion.2 = f32[256,1536]{1,0:T(8,128)} fusion(bf16[256,2048]{1,0:T(8,128)(2,1)} %fusion.15, bf16[2048,3072]{1,0:T(8,128)(2,1)} %all-gather.5.cloned.1.call-done), kind=kOutput, calls=%fused_computation.2 | convolution fusion | flops 1610612736 | bytes 8912896 | tf_op jit(solution)/shard_map/dot_general | solution.py:122
  421.9 8.8 %convolution_convert_fusion.1 = bf16[256,2048]{1,0:T(8,128)(2,1)S(1)} fusion(bf16[1536,2048]{0,1:T(8,128)(2,1)} %bitcast.14, bf16[256,2048]{1,0:T(8,128)(2,1)} %fusion.15, bf16[2048,3072]{1,0:T(8,128)(2,1)} %all-gather.5.cloned.1.call-done, f32[256,1536]{1,0:T(8,128)} %fusion.2), kind=kOutput, calls=%fused_computation.7 | convolution fusion | flops 3224109056 | bytes 16252928 | tf_op jit(solution)/shard_map/dot_general | solution.py:128
  430.7 17.4 %all_to_all.33 = bf16[2,128,2048]{2,1,0:T(8,128)(2,1)S(1)} all-to-all(bf16[2,128,2048]{2,1,0:T(8,128)(2,1)S(1)} %bitcast.57), channel_id=1, replica_groups=mesh['rep'=2,'fs'=32,'tp'=2] {'tp'}, dimensions={0} | all-to-all | bytes 2097152 | tf_op jit(solution)/shard_map/all_to_all | solution.py:52
  448.3 1.0 fusion.42
  (46 shorter events, 5.4 us)
Async XLA Ops:
  6.5 156.4 %copy-start = (f32[31,512]{1,0:T(8,128)S(1)}, f32[31,512]{1,0:T(8,128)}, u32[]{:S(2)}) copy-start(f32[31,512]{1,0:T(8,128)} %param.15) | copy-start | bytes 190468
  6.5 152.2 %all-gather.3.cloned.1.call-start = ((), (), s32[]{:S(2)}) async-start(), calls=%async_computation.6 | async-start | bytes 4325376 | tf_op jit(solution)/shard_map/all_gather | solution.py:38
  8.1 407.6 %all-gather.5.cloned.1.call-start = ((), (), s32[]{:S(2)}) async-start(), calls=%async_computation.7 | async-start | bytes 12976128 | tf_op jit(solution)/shard_map/all_gather | solution.py:38
  10.0 6.8 %copy-start.4 = (bf16[512,64]{0,1:T(8,128)(2,1)S(1)}, bf16[512,64]{0,1:T(8,128)(2,1)}, u32[]{:S(2)}) copy-start(bf16[512,64]{0,1:T(8,128)(2,1)} %param.17) | copy-start | bytes 196612
  18.4 8.9 %copy-start.5 = (f32[2048]{0:T(1024)S(1)}, f32[2048]{0:T(1024)}, u32[]{:S(2)}) copy-start(f32[2048]{0:T(1024)} %param.12) | copy-start | bytes 24580
  18.4 152.5 %all-to-all-start.1 = ((bf16[32,512,64]{1,2,0:T(8,128)(2,1)}), bf16[32,512,64]{1,2,0:T(8,128)(2,1)S(1)}, u32[]{:S(2)}, u32[]{:S(2)}) async-start(bf16[32,512,64]{1,2,0:T(8,128)(2,1)} %broadcast_in_dim.13), calls=%async_computation.1 | async-start | bytes 4194304 | tf_op jit(solution)/shard_map/all_to_all | solution.py:20
  28.7 132.9 %copy-start.2 = (bf16[256,2048]{1,0:T(8,128)(2,1)S(1)}, bf16[256,2048]{1,0:T(8,128)(2,1)}, u32[]{:S(2)}) copy-start(bf16[256,2048]{1,0:T(8,128)(2,1)} %fusion.17) | copy-start | bytes 3145732
  158.7 3.1 copy-start.8
  162.6 0.7 copy-start.9
  166.9 3.3 copy-start.7
  171.7 23.6 %copy-start.1 = (bf16[128,1,2048]{2,0,1:T(8,128)(2,1)S(1)}, bf16[128,1,2048]{2,0,1:T(8,128)(2,1)}, u32[]{:S(2)}) copy-start(bf16[128,1,2048]{2,0,1:T(8,128)(2,1)} %param.11) | copy-start | bytes 1572868
  195.4 4.7 %copy-start.3 = (bf16[1536,64]{0,1:T(8,128)(2,1)S(1)}, bf16[1536,64]{0,1:T(8,128)(2,1)}, u32[]{:S(2)}) copy-start(bf16[1536,64]{0,1:T(8,128)(2,1)} %param.21) | copy-start | bytes 589828
  203.5 7.7 %copy-start.6 = (f32[2048]{0:T(1024)S(1)}, f32[2048]{0:T(1024)}, u32[]{:S(2)}) copy-start(f32[2048]{0:T(1024)} %param.18) | copy-start | bytes 24580
  203.5 218.4 %all-to-all-start.4 = ((bf16[32,1536,64]{1,2,0:T(8,128)(2,1)}), bf16[32,1536,64]{1,2,0:T(8,128)(2,1)}, u32[]{:S(2)}, u32[]{:S(2)}) async-start(bf16[32,1536,64]{1,2,0:T(8,128)(2,1)} %stack.2), calls=%async_computation.4 | async-start | bytes 12582912 | tf_op jit(solution)/shard_map/all_to_all | solution.py:14
Sparse Core Ops, SparseCore 0:
  9.0 149.7 all-gather.2
  160.4 255.3 all-gather.4
